TPU v7x, 256 devices: a whole 4x4x8 slice. The times are simulated.
256 devices in a mesh: fs: 16 (over y, x), tp: 16 (over z, core).
Axes of the slice: x: 4, y: 4, z: 8, core: 2. Of those that a mesh axis runs over, the one named last changes fastest.
Arguments:
- tokens: bfloat16 [32768, 2048], P(('fs', 'tp')), may hold values from -6 to 6
- norm_gain: float32 [2048], replicated, may hold values from 0.1 to 1.9
- gate_weight: bfloat16 [2048, 5632], P('fs', 'tp'), may hold values from -0.125 to 0.125
- up_weight: bfloat16 [2048, 5632], P('fs', 'tp'), may hold values from -0.125 to 0.125
- down_weight: bfloat16 [5632, 2048], P('tp', 'fs'), may hold values from -0.078125 to 0.078125
Outputs:
- mixed: bfloat16 [32768, 2048], P(('fs', 'tp'))
All inputs are finite; a program needn't handle non-finite values.
Results may differ from a plain program's by a relative error of at most 0.0065.
Values may be sent and summed in bfloat16 or wider, within the bound.
A program may use at most 128 MiB of HBM per device.

v0:
```python
import jax
import jax.numpy as jnp
from jax import lax
from jax.sharding import PartitionSpec as P

eps_floor = 0.05


def sent_together(arrays, axis, dim, along):
    both = jnp.concatenate(arrays, axis=along)
    out, at, outs = (lax.all_gather(both, axis, axis=dim, tiled=True), 0, [])
    for a in arrays:
        outs.append(lax.slice_in_dim(out, at, at + a.shape[along], axis=along))
        at += a.shape[along]
    return tuple(outs)


def joined_along(blocks, dim):
    blocks = jnp.moveaxis(blocks, 0, dim)
    lengths = blocks.shape
    return blocks.reshape(*lengths[:dim], lengths[dim] * lengths[dim + 1], *lengths[dim + 2 :])


def from_everyone(x, axis):
    length = lax.axis_size(axis)
    return lax.all_to_all(jnp.broadcast_to(x[None], (length, *x.shape)), axis, 0, 0, tiled=True)


def collect(x, axis, dim):
    return joined_along(from_everyone(x, axis), dim)


def local(tokens, norm_gain, gate_weight, up_weight, down_weight):
    values = tokens.astype(jnp.float32)
    factor = lax.rsqrt(jnp.mean(values * values, axis=-1, keepdims=True) + eps_floor)
    normed = (values * factor * norm_gain).astype(jnp.bfloat16)
    gate_full, upper_full = sent_together((gate_weight, up_weight), "fs", 0, 1)
    piece = lax.all_gather(normed, "tp", axis=0, tiled=True)
    gate = jnp.dot(piece, gate_full, preferred_element_type=jnp.float32)
    upper = jnp.dot(piece, upper_full, preferred_element_type=jnp.float32)
    hidden = (jax.nn.silu(gate) * upper).astype(jnp.bfloat16)
    down_local = collect(down_weight, "fs", 1)
    mixed = lax.psum_scatter(
        jnp.dot(hidden, down_local, preferred_element_type=jnp.float32),
        "tp",
        scatter_dimension=0,
        tiled=True,
    )
    return mixed.astype(jnp.bfloat16)


def solution(mesh):
    return jax.shard_map(
        local,
        mesh=mesh,
        in_specs=(P(("fs", "tp"), None), P(), P("fs", "tp"), P("fs", "tp"), P("tp", "fs")),
        out_specs=P(("fs", "tp"), None),
        check_vma=False,
    )
```

profile of v0, /device:TPU:2, one launch (start us, length us, event | category | flops | bytes accessed | tf_op | source)
XLA Modules:
  0.0 261.6 jit_solution(3198704871677870176)
XLA Ops:
  6.5 0.0 all-gather.5.cloned.1.call-start
  6.5 1.6 pad_maximum_fusion
  8.1 0.0 all-gather.5.cloned.1.call-update
  8.2 0.0 all-gather.3.cloned.1.call-start
  8.2 1.2 fusion.7
  9.5 2.0 fusion.9
  11.5 0.0 all-gather.3.cloned.1.call-update
  11.5 2.2 broadcast_in_dim.2
  13.7 7.5 %all-to-all-start = ((bf16[16,352,128]{2,1,0:T(8,128)(2,1)}), bf16[16,352,128]{2,1,0:T(8,128)(2,1)S(1)}, u32[]{:S(2)}, u32[]{:S(2)}) async-start(bf16[16,352,128]{2,1,0:T(8,128)(2,1)} %broadcast_in_dim.2), calls=%async_computation | async-start | bytes 2883584 | tf_op jit(solution)/shard_map/all_to_all | solution.py:26
  21.2 0.0 reduce-scatter.2.cloned.1.call-start
  21.2 56.4 %all-gather.5.cloned.1.call-done = bf16[2048,704]{0,1:T(8,128)(2,1)} async-done(((bf16[128,704]{0,1:T(8,128)(2,1)}), bf16[2048,704]{0,1:T(8,128)(2,1)}) %all-gather.5.cloned.1.call-update) | async-done | bytes 2883600 | tf_op jit(solution)/shard_map/all_gather | solution.py:11
  77.6 57.4 %all-gather.3.cloned.1.call-done = bf16[2048,2048]{1,0:T(8,128)(2,1)} async-done(((bf16[128,2048]{1,0:T(8,128)(2,1)}), bf16[2048,2048]{1,0:T(8,128)(2,1)}) %all-gather.3.cloned.1.call-update) | async-done | bytes 8388624 | tf_op jit(solution)/shard_map/all_gather | solution.py:38
  135.0 0.0 copy-start
  135.0 0.0 copy-start.1
  135.0 6.4 %fusion.5 = f32[2048,352]{0,1:T(8,128)S(1)} fusion(bf16[2048,2048]{1,0:T(8,128)(2,1)} %all-gather.3.cloned.1.call-done, bf16[2048,704]{0,1:T(8,128)(2,1)} %all-gather.5.cloned.1.call-done), kind=kOutput, calls=%fused_computation.6 | convolution fusion | flops 2952790016 | bytes 12713984 | tf_op jit(solution)/shard_map/dot_general | solution.py:39
  141.5 0.0 copy-done
  141.5 0.6 copy-done.1
  142.1 3.5 %fusion = bf16[2048,352]{0,1:T(8,128)(2,1)S(1)} fusion(bf16[2048,2048]{1,0:T(8,128)(2,1)S(1)} %copy-done, f32[2048,352]{0,1:T(8,128)S(1)} %fusion.5, bf16[2048,704]{0,1:T(8,128)(2,1)S(1)} %copy-done.1), kind=kOutput, calls=%fused_computation.1 | convolution fusion | flops 2957115392 | bytes 14155776 | tf_op jit(solution)/shard_map/dot_general | solution.py:40
  145.6 0.0 all-to-all-done
  145.6 8.1 %fusion.1 = f32[2048,2048]{1,0:T(8,128)} fusion(bf16[2048,352]{0,1:T(8,128)(2,1)S(1)} %fusion, bf16[16,352,128]{2,1,0:T(8,128)(2,1)S(1)} %all-to-all-done), kind=kOutput, calls=%fused_computation.2 | convolution fusion | flops 2952790016 | bytes 19660800 | tf_op jit(solution)/shard_map/dot_general | solution.py:44
  153.7 0.0 reduce-scatter.2.cloned.1.call-update
  153.8 99.3 %reduce-scatter.2.cloned.1.call-done = f32[128,2048]{1,0:T(8,128)} async-done(((f32[2048,2048]{1,0:T(8,128)}), f32[128,2048]{1,0:T(8,128)}) %reduce-scatter.2.cloned.1.call-update) | async-done | bytes 1048592 | tf_op jit(solution)/shard_map/reduce_scatter | solution.py:43
  253.0 2.1 convert_element_type.15
  (1 shorter events, 0.0 us)
Async XLA Ops:
  6.5 71.1 %all-gather.5.cloned.1.call-start = ((), (), s32[]{:S(2)}) async-start(), calls=%async_computation.3 | async-start | bytes 3063808 | tf_op jit(solution)/shard_map/all_gather | solution.py:11
  8.2 126.8 %all-gather.3.cloned.1.call-start = ((), (), s32[]{:S(2)}) async-start(), calls=%async_computation.2 | async-start | bytes 8912896 | tf_op jit(solution)/shard_map/all_gather | solution.py:38
  13.7 131.9 %all-to-all-start = ((bf16[16,352,128]{2,1,0:T(8,128)(2,1)}), bf16[16,352,128]{2,1,0:T(8,128)(2,1)S(1)}, u32[]{:S(2)}, u32[]{:S(2)}) async-start(bf16[16,352,128]{2,1,0:T(8,128)(2,1)} %broadcast_in_dim.2), calls=%async_computation | async-start | bytes 2883584 | tf_op jit(solution)/shard_map/all_to_all | solution.py:26
  21.2 231.8 %reduce-scatter.2.cloned.1.call-start = ((), (), s32[]{:S(2)}) async-start(), calls=%async_computation.4 | async-start | bytes 17825792 | tf_op jit(solution)/shard_map/reduce_scatter | solution.py:43
  135.0 6.4 %copy-start = (bf16[2048,2048]{1,0:T(8,128)(2,1)S(1)}, bf16[2048,2048]{1,0:T(8,128)(2,1)}, u32[]{:S(2)}) copy-start(bf16[2048,2048]{1,0:T(8,128)(2,1)} %all-gather.3.cloned.1.call-done) | copy-start | bytes 25165828
  135.0 7.1 %copy-start.1 = (bf16[2048,704]{0,1:T(8,128)(2,1)S(1)}, bf16[2048,704]{0,1:T(8,128)(2,1)}, u32[]{:S(2)}) copy-start(bf16[2048,704]{0,1:T(8,128)(2,1)} %all-gather.5.cloned.1.call-done) | copy-start | bytes 8650756
Sparse Core Ops, SparseCore 0:
  9.7 67.8 all-gather.4
  79.4 55.5 all-gather.2
  153.9 99.0 reduce-scatter.1
where the time goes:
time: 262 us
  waiting for transfers between devices  213 us (81%)
  matrix products  18.1 us (7%)
  between operations  13.1 us (5%)
  starting transfers between devices  7.56 us (3%)
  other arithmetic  6.96 us (3%)
  local copies, waits for them, and re-layouts  2.83 us (1%)
    reduce_scatter x1, waiting for transfers between devices, local(): lax.psum_scatter(jnp.dot(hidden, down_local, preferred_element_type=jnp.f...  99.3 us
    all_gather x1, waiting for transfers between devices, local(): piece = lax.all_gather(normed, 'tp', axis=0, tiled=True)  57.4 us
    all_gather x1, waiting for transfers between devices, sent_together(): out, at, outs = (lax.all_gather(both, axis, axis=dim, tiled=True), 0, [])  56.4 us
    dot_general x1, matrix products, local(): jnp.dot(hidden, down_local, preferred_element_type=jnp.float32)  8.11 us
    all_to_all x1, starting transfers between devices, from_everyone(): lax.all_to_all(jnp.broadcast_to(x[None], (length, *x.shape)), axis, 0, 0,...  7.48 us
    dot_general x1, matrix products, local(): gate = jnp.dot(piece, gate_full, preferred_element_type=jnp.float32)  6.43 us
  transfers between devices with their start and end apart: 4, of which 3 were waited for; matrix products, arithmetic and copies ran while one was open for 6% of the time, Pallas kernels for 0%

commit v1 on v0

--- a/solution.py
+++ b/solution.py
@@ -35,7 +35,9 @@
     factor = lax.rsqrt(jnp.mean(values * values, axis=-1, keepdims=True) + eps_floor)
     normed = (values * factor * norm_gain).astype(jnp.bfloat16)
     gate_full, upper_full = sent_together((gate_weight, up_weight), "fs", 0, 1)
-    piece = lax.all_gather(normed, "tp", axis=0, tiled=True)
+    piece = jnp.concatenate(
+        lax.all_to_all(jnp.stack([normed] * lax.axis_size("tp")), "tp", 0, 0), axis=0
+    )
     gate = jnp.dot(piece, gate_full, preferred_element_type=jnp.float32)
     upper = jnp.dot(piece, upper_full, preferred_element_type=jnp.float32)
     hidden = (jax.nn.silu(gate) * upper).astype(jnp.bfloat16)

time: 262 us -> 351 us (1.34)
  waiting for transfers between devices: 213 us -> 289 us
  starting transfers between devices: 7.56 us -> 16.3 us
    all_to_all x0 -> x1, waiting for transfers between devices: none -> 183 us  [local(): lax.all_to_all(jnp.stack([normed] * lax.axis_size('tp')), 'tp', 0, 0)]
    all_gather x1 -> x0, waiting for transfers between devices: 57.4 us -> none  [local(): piece = lax.all_gather(normed, 'tp', axis=0, tiled=True)]
    all_gather x1, waiting for transfers between devices: 56.4 us -> 0.02 us  [sent_together(): out, at, outs = (lax.all_gather(both, axis, axis=dim, tiled=True), 0, [])]
    all_to_all x0 -> x1, starting transfers between devices: none -> 8.75 us  [local(): lax.all_to_all(jnp.stack([normed] * lax.axis_size('tp')), 'tp', 0, 0)]
    all_to_all x1, waiting for transfers between devices: 0.01 us -> 6.68 us  [from_everyone(): lax.all_to_all(jnp.broadcast_to(x[None], (length, *x.shape)), axis, 0, 0,...]
    another operation x0 -> x1, local copies, waits for them, and re-layouts: none -> 4.31 us  [local(): jnp.stack([normed] * lax.axis_size('tp'))]
  transfers between devices with their start and end apart: 4 -> 4, of which waited for: 3 -> 3; matrix products, arithmetic and copies ran while one was open for 6% -> 4% of each run, Pallas kernels for 0% -> 0%
where the time goes in v1:
time: 351 us
  waiting for transfers between devices  289 us (82%)
  matrix products  21.2 us (6%)
  starting transfers between devices  16.3 us (5%)
  between operations  13.5 us (4%)
  local copies, waits for them, and re-layouts  5.68 us (2%)
  other arithmetic  5.24 us (1%)
    all_to_all x1, waiting for transfers between devices, local(): lax.all_to_all(jnp.stack([normed] * lax.axis_size('tp')), 'tp', 0, 0)  183 us
    reduce_scatter x1, waiting for transfers between devices, local(): lax.psum_scatter(jnp.dot(hidden, down_local, preferred_element_type=jnp.f...  98.6 us
    all_to_all x1, starting transfers between devices, local(): lax.all_to_all(jnp.stack([normed] * lax.axis_size('tp')), 'tp', 0, 0)  8.75 us
    dot_general x1, matrix products, local(): jnp.dot(hidden, down_local, preferred_element_type=jnp.float32)  8.18 us
    all_to_all x1, starting transfers between devices, from_everyone(): lax.all_to_all(jnp.broadcast_to(x[None], (length, *x.shape)), axis, 0, 0,...  7.48 us
  transfers between devices with their start and end apart: 4, of which 3 were waited for; matrix products, arithmetic and copies ran while one was open for 4% of the time, Pallas kernels for 0%

profile of v1, /device:TPU:2, one launch (start us, length us, event | category | flops | bytes accessed | tf_op | source)
XLA Modules:
  0.0 350.7 jit_solution(3526202078781301542)
XLA Ops:
  6.5 1.2 fusion.7
  7.8 1.2 fusion.9
  9.0 4.3 %stack.2 = bf16[16,128,2048]{2,1,0:T(8,128)(2,1)} broadcast(bf16[128,2048]{1,0:T(8,128)(2,1)S(1)} %fusion.9), dimensions={1,2} | broadcast | bytes 8912896 | tf_op jit(solution)/shard_map/stack | solution.py:39
  13.3 8.8 %all-to-all-start = ((bf16[16,128,2048]{2,1,0:T(8,128)(2,1)}), bf16[16,128,2048]{2,1,0:T(8,128)(2,1)}, u32[]{:S(2)}, u32[]{:S(2)}) async-start(bf16[16,128,2048]{2,1,0:T(8,128)(2,1)} %stack.2), calls=%async_computation | async-start | bytes 16777216 | tf_op jit(solution)/shard_map/all_to_all | solution.py:39
  22.1 0.0 all-gather.2.cloned.1.call-start
  22.1 0.0 copy-done
  22.1 0.0 copy-done.1
  22.2 0.7 pad_maximum_fusion
  22.8 0.0 all-gather.2.cloned.1.call-update
  22.9 183.4 %all-to-all-done = bf16[16,128,2048]{2,1,0:T(8,128)(2,1)} async-done(((bf16[16,128,2048]{2,1,0:T(8,128)(2,1)}), bf16[16,128,2048]{2,1,0:T(8,128)(2,1)}, u32[]{:S(2)}, u32[]{:S(2)}) %all-to-all-start) | async-done | bytes 8388640 | tf_op jit(solution)/shard_map/all_to_all | solution.py:39
  206.3 0.0 copy-done.2
  206.3 1.4 broadcast_in_dim.2
  207.7 7.5 %all-to-all-start.1 = ((bf16[16,352,128]{2,1,0:T(8,128)(2,1)}), bf16[16,352,128]{2,1,0:T(8,128)(2,1)S(1)}, u32[]{:S(2)}, u32[]{:S(2)}) async-start(bf16[16,352,128]{2,1,0:T(8,128)(2,1)} %broadcast_in_dim.2), calls=%async_computation.1 | async-start | bytes 2883584 | tf_op jit(solution)/shard_map/all_to_all | solution.py:26
  215.1 0.0 reduce-scatter.2.cloned.1.call-start
  215.2 0.0 all-gather.2.cloned.1.call-done
  215.2 0.0 copy-start.3
  215.2 6.2 %fusion.5 = f32[2048,352]{0,1:T(8,128)S(1)} fusion(bf16[2048,2048]{1,0:T(8,128)(2,1)} %bitcast, bf16[2048,704]{0,1:T(8,128)(2,1)} %all-gather.2.cloned.1.call-done), kind=kOutput, calls=%fused_computation.6 | convolution fusion | flops 2952790016 | bytes 12713984 | tf_op jit(solution)/shard_map/dot_general | solution.py:41
  221.4 0.0 copy-done.3
  221.4 6.8 %fusion = bf16[2048,352]{0,1:T(8,128)(2,1)S(1)} fusion(bf16[2048,2048]{1,0:T(8,128)(2,1)} %bitcast, f32[2048,352]{0,1:T(8,128)S(1)} %fusion.5, bf16[2048,704]{0,1:T(8,128)(2,1)S(1)} %copy-done.3), kind=kOutput, calls=%fused_computation.1 | convolution fusion | flops 2957115392 | bytes 14155776 | tf_op jit(solution)/shard_map/dot_general | solution.py:42
  228.3 6.7 %all-to-all-done.1 = bf16[16,352,128]{2,1,0:T(8,128)(2,1)S(1)} async-done(((bf16[16,352,128]{2,1,0:T(8,128)(2,1)}), bf16[16,352,128]{2,1,0:T(8,128)(2,1)S(1)}, u32[]{:S(2)}, u32[]{:S(2)}) %all-to-all-start.1) | async-done | bytes 1441824 | tf_op jit(solution)/shard_map/all_to_all | solution.py:26
  234.9 8.2 %fusion.1 = f32[2048,2048]{1,0:T(8,128)} fusion(bf16[2048,352]{0,1:T(8,128)(2,1)S(1)} %fusion, bf16[16,352,128]{2,1,0:T(8,128)(2,1)S(1)} %all-to-all-done.1), kind=kOutput, calls=%fused_computation.2 | convolution fusion | flops 2952790016 | bytes 19660800 | tf_op jit(solution)/shard_map/dot_general | solution.py:46
  243.1 0.0 reduce-scatter.2.cloned.1.call-update
  243.1 98.6 %reduce-scatter.2.cloned.1.call-done = f32[128,2048]{1,0:T(8,128)} async-done(((f32[2048,2048]{1,0:T(8,128)}), f32[128,2048]{1,0:T(8,128)}) %reduce-scatter.2.cloned.1.call-update) | async-done | bytes 1048592 | tf_op jit(solution)/shard_map/reduce_scatter | solution.py:45
  341.8 2.1 convert_element_type.15
  (4 shorter events, 0.0 us)
Async XLA Ops:
  13.3 8.8 %copy-start = (bf16[128,352]{0,1:T(8,128)(2,1)S(1)}, bf16[128,352]{0,1:T(8,128)(2,1)}, u32[]{:S(2)}) copy-start(bf16[128,352]{0,1:T(8,128)(2,1)} %param.8) | copy-start | bytes 270340
  13.3 8.8 %copy-start.1 = (bf16[128,352]{0,1:T(8,128)(2,1)S(1)}, bf16[128,352]{0,1:T(8,128)(2,1)}, u32[]{:S(2)}) copy-start(bf16[128,352]{0,1:T(8,128)(2,1)} %param.7) | copy-start | bytes 270340
  13.3 193.0 %copy-start.2 = (bf16[352,128]{1,0:T(8,128)(2,1)S(1)}, bf16[352,128]{1,0:T(8,128)(2,1)}, u32[]{:S(2)}) copy-start(bf16[352,128]{1,0:T(8,128)(2,1)} %param.9) | copy-start | bytes 270340
  13.3 193.0 %all-to-all-start = ((bf16[16,128,2048]{2,1,0:T(8,128)(2,1)}), bf16[16,128,2048]{2,1,0:T(8,128)(2,1)}, u32[]{:S(2)}, u32[]{:S(2)}) async-start(bf16[16,128,2048]{2,1,0:T(8,128)(2,1)} %stack.2), calls=%async_computation | async-start | bytes 16777216 | tf_op jit(solution)/shard_map/all_to_all | solution.py:39
  22.1 193.1 %all-gather.2.cloned.1.call-start = ((), (), s32[]{:S(2)}) async-start(), calls=%async_computation.3 | async-start | bytes 3063808 | tf_op jit(solution)/shard_map/all_gather | solution.py:11
  207.7 27.3 %all-to-all-start.1 = ((bf16[16,352,128]{2,1,0:T(8,128)(2,1)}), bf16[16,352,128]{2,1,0:T(8,128)(2,1)S(1)}, u32[]{:S(2)}, u32[]{:S(2)}) async-start(bf16[16,352,128]{2,1,0:T(8,128)(2,1)} %broadcast_in_dim.2), calls=%async_computation.1 | async-start | bytes 2883584 | tf_op jit(solution)/shard_map/all_to_all | solution.py:26
  215.1 126.6 %reduce-scatter.2.cloned.1.call-start = ((), (), s32[]{:S(2)}) async-start(), calls=%async_computation.4 | async-start | bytes 17825792 | tf_op jit(solution)/shard_map/reduce_scatter | solution.py:45
  215.2 6.2 %copy-start.3 = (bf16[2048,704]{0,1:T(8,128)(2,1)S(1)}, bf16[2048,704]{0,1:T(8,128)(2,1)}, u32[]{:S(2)}) copy-start(bf16[2048,704]{0,1:T(8,128)(2,1)} %all-gather.2.cloned.1.call-done) | copy-start | bytes 8650756
Sparse Core Ops, SparseCore 0:
  25.3 56.8 all-gather.1
  243.3 98.4 reduce-scatter.1
